TPU v7x, 512 devices: a 4x2x32 block of a 4x8x32 slice. The times are simulated.
512 devices in a mesh: grp: 2 (over y), fs: 64 (over z, core), tp: 4 (over x).
Axes of the slice: x: 4, y: 2, z: 32, core: 2. Of those that a mesh axis runs over, the one named last changes fastest.
The devices are a block of a 4x8x32 slice.
Arguments:
- tokens: bfloat16 [28672, 2048], P(('grp', 'fs'), 'tp'), parts along dimension 0, may hold values from -6 to 6
- route_ids: int32 [28672, 2], P(('grp', 'fs')), parts along dimension 0, may hold values from 0 to 63, all different within a row; in each aligned block of 224 rows (0 to 223, 224 to 447, ...) at most 10 rows name the same one
- route_weights: float32 [28672, 2], P(('grp', 'fs')), parts along dimension 0, may hold values from 0.25 to 1
- norm_gain: float32 [2048], P('fs'), may hold values from 0.1 to 1.9
- gate_master: float32 [64, 2048, 512], P(None, 'fs', 'tp'), may hold values from -0.125 to 0.125
- up_master: float32 [64, 2048, 512], P(None, 'fs', 'tp'), may hold values from -0.125 to 0.125
- down_master: float32 [64, 2048, 512], P(None, 'fs', 'tp'), may hold values from -0.25 to 0.25
Outputs:
- gate_serve: bfloat16 [128, 2048, 512], P(('grp', 'fs'), None, 'tp'), parts along dimension 0
- up_serve: bfloat16 [128, 2048, 512], P(('grp', 'fs'), None, 'tp'), parts along dimension 0
- down_serve: bfloat16 [128, 2048, 512], P(('grp', 'fs'), None, 'tp'), parts along dimension 0
- moe_output: bfloat16 [28672, 2048], P(('grp', 'fs'), 'tp'), parts along dimension 0
There are 2 independent parts, one for each index of `grp`. A program takes and returns all parts, laid end to end along the dimension named above; an argument that names none is the same for every part. Nothing has to cross between parts.
Inputs may be any that keep to these rules, and one draw needn't show every extreme that they name: `route_ids`: the 2 experts of a row differ; within the rows of one index of fs (aligned blocks of 224 rows) no expert is named more than 10 times.
All inputs are finite; a program needn't handle non-finite values.
Results may differ from a plain program's by a relative error of at most 0.012.
Values may be sent and summed in bfloat16 or wider, within the bound.
A program may use at most 64 MiB of HBM per device.

v0:
```python
import jax
import jax.numpy as jnp
from jax import lax
from jax.sharding import Mesh
from jax.sharding import PartitionSpec as P

FS = ("fs_0", "fs_1")
GRP_FS = ("grp", "fs_0", "fs_1")


norm_epsilon = 1e-06


def side_by_side(arrays, axis, split_dim, concat_dim, along):
    widths = [a.shape[along] for a in arrays]
    both = jnp.concatenate(arrays, axis=along)
    filled = lax.all_to_all(both, axis, split_axis=split_dim, concat_axis=concat_dim, tiled=True)
    return tuple(jnp.split(filled, [sum(widths[:k]) for k in range(1, len(widths))], axis=along))


def from_everyone(value, axis):
    copies = jnp.broadcast_to(value, (lax.axis_size(axis), *value.shape))
    return lax.all_to_all(copies, axis, split_axis=0, concat_axis=0, tiled=True)


def of_everyone(value, axis):
    everything = from_everyone(value, axis)
    return jnp.sum(everything, axis=0)


def in_blocks(value, dim, size):
    before, after = (value.shape[:dim], value.shape[dim + 1 :])
    return jnp.moveaxis(value.reshape(*before, size, -1, *after), dim, 0)


def laid_out(blocks, dim):
    blocks = jnp.moveaxis(blocks, 0, dim)
    lengths = blocks.shape
    return blocks.reshape(*lengths[:dim], lengths[dim] * lengths[dim + 1], *lengths[dim + 2 :])


def exchange_in_order(blocks, axes, turns):
    inside = blocks.shape[1:]
    filled = blocks.reshape(*(lax.axis_size(a) for a in axes), *inside)
    for k in turns:
        filled = lax.all_to_all(filled, axes[k], k, k, tiled=True)
    return filled.reshape(-1, *inside)


def two_step_exchange(value, groups, turns, split_dim, concat_dim):
    size = lax.axis_size(groups[0]) * lax.axis_size(groups[1])
    blocks = in_blocks(value, split_dim, size)
    return laid_out(exchange_in_order(blocks, groups, turns), concat_dim)


def gather_directly(value, axis, dim):
    return laid_out(from_everyone(value, axis), dim)


def slot_numbers(route_ids, experts, capacity):
    flat_ids = route_ids.reshape(-1)
    onehot = (flat_ids[:, None] == jnp.arange(experts, dtype=jnp.int32)[None, :]).astype(jnp.int32)
    before = jnp.cumsum(onehot, axis=0) - onehot
    position = jnp.sum(before * onehot, axis=1)
    return (flat_ids * capacity + position).reshape(route_ids.shape)


def local(tokens, route_ids, route_weights, norm_gain, gate_master, up_master, down_master):
    experts = gate_master.shape[0]
    shards = lax.axis_size(FS)
    columns = lax.axis_size("tp")
    per_device = experts // shards
    tok_rows = route_ids.shape[0]
    top_count = route_ids.shape[1]
    local_width = tokens.shape[1]
    model_width = local_width * columns
    capacity = max(2, 3 * tok_rows * top_count // (2 * experts))
    row_gain = norm_gain[None, :, None]
    gate_half = (gate_master * row_gain).astype(jnp.bfloat16)
    up_half = (up_master * row_gain).astype(jnp.bfloat16)
    down_half = down_master.astype(jnp.bfloat16)
    gate_serve, up_serve, down_serve = side_by_side((gate_half, up_half, down_half), FS, 0, 1, 2)
    slot_ids = slot_numbers(route_ids, experts, capacity)
    slot_range = jnp.arange(experts * capacity, dtype=jnp.int32)
    selects = [
        (slot_ids[:, rank_slot, None] == slot_range[None, :]).astype(jnp.bfloat16)
        for rank_slot in range(top_count)
    ]
    placing = selects[0]
    for extra in selects[1:]:
        placing = placing + extra
    local_values = tokens.astype(jnp.float32)
    squares = of_everyone(jnp.sum(local_values * local_values, axis=1), "tp")
    inverse = lax.rsqrt(squares / model_width + norm_epsilon)[:, None]
    normed = (local_values * inverse).astype(jnp.bfloat16)
    buffer = jnp.einsum("ts,td->sd", placing, normed, preferred_element_type=jnp.float32).astype(
        jnp.bfloat16
    )
    arrived = two_step_exchange(
        buffer.reshape(shards, per_device * capacity, local_width), ("fs_0", "fs_1"), (1, 0), 0, 0
    )
    arrived = arrived.reshape(shards, per_device, capacity, local_width)
    partial_value = gather_directly(arrived, "tp", 3)
    gate_sum = jnp.einsum(
        "sxcd,xdf->xscf", partial_value, gate_serve, preferred_element_type=jnp.float32
    )
    up_sum = jnp.einsum(
        "sxcd,xdf->xscf", partial_value, up_serve, preferred_element_type=jnp.float32
    )
    hidden = (jax.nn.silu(gate_sum) * up_sum).astype(jnp.bfloat16)
    unit_block = hidden.shape[3]
    hidden_all = gather_directly(hidden, "tp", 3)
    down_cols = lax.all_to_all(down_serve, "tp", split_axis=1, concat_axis=2, tiled=True)
    hidden_parts = hidden_all.reshape(per_device, shards, capacity, columns, unit_block)
    down_parts = down_cols.reshape(per_device, local_width, columns, unit_block)
    partial_value = jnp.einsum(
        "xscpf,xdpf->pdsxc", hidden_parts, down_parts, preferred_element_type=jnp.float32
    )
    rounded = lax.optimization_barrier(partial_value.astype(jnp.bfloat16)).astype(jnp.float32)
    summed = (
        jnp.sum(rounded, axis=0)
        .reshape(local_width, shards * per_device * capacity)
        .astype(jnp.bfloat16)
    )
    returned = lax.all_to_all(
        summed.reshape(local_width, shards, per_device * capacity),
        FS,
        split_axis=1,
        concat_axis=1,
        tiled=True,
    )
    returned = returned.reshape(local_width, experts * capacity)
    combined = jnp.zeros((tok_rows, local_width), jnp.float32)
    for rank_slot in range(top_count):
        picked = jnp.einsum(
            "ts,ds->td", selects[rank_slot], returned, preferred_element_type=jnp.float32
        )
        combined = combined + route_weights[:, rank_slot : rank_slot + 1] * picked
    return (gate_serve, up_serve, down_serve, combined.astype(jnp.bfloat16))


def solution(mesh):
    torus = Mesh(
        mesh.devices.reshape(mesh.shape["grp"], 32, 2, mesh.shape["tp"]),
        ("grp", "fs_0", "fs_1", "tp"),
    )
    placed = (
        P(GRP_FS, "tp"),
        P(GRP_FS, None),
        P(GRP_FS, None),
        P(FS),
        P(None, FS, "tp"),
        P(None, FS, "tp"),
        P(None, FS, "tp"),
    )
    return jax.shard_map(
        local,
        mesh=torus,
        in_specs=placed,
        out_specs=(
            P(GRP_FS, None, "tp"),
            P(GRP_FS, None, "tp"),
            P(GRP_FS, None, "tp"),
            P(GRP_FS, "tp"),
        ),
        check_vma=False,
    )
```

profile of v0, /device:TPU:33, one launch (start us, length us, event | category | flops | bytes accessed | tf_op | source)
XLA Modules:
  0.0 512.1 jit_solution(14046759189263784657)
XLA Ops:
  0.6 1.1 fusion.9
  2.3 5.1 all-to-all-start.2
  8.4 1.2 reduce-window.6
  11.6 1.4 convolution_convert_fusion
  13.6 44.6 %all_to_all.58 = bf16[32,2,1,10,512]{4,0,3,2,1:T(8,128)(2,1)S(1)} all-to-all(bf16[32,2,1,10,512]{4,0,3,2,1:T(8,128)(2,1)S(1)} %copy.90), channel_id=1, replica_groups=mesh['grp'=2,'fs_0'=32,'fs_1'=2,'tp'=4] {'fs_1'}, dimensions={1} | all-to-all | bytes 1310720 | tf_op jit(solution)/shard_map/all_to_all | solution.py:46
  58.9 81.5 %all_to_all.59 = bf16[32,2,1,10,512]{4,1,3,2,0:T(2,128)(2,1)S(1)} all-to-all(bf16[32,2,1,10,512]{4,1,3,2,0:T(2,128)(2,1)S(1)} %copy.91), channel_id=1, replica_groups=mesh['grp'=2,'fs_0'=32,'fs_1'=2,'tp'=4] {'fs_0'}, dimensions={0} | all-to-all | bytes 1310720 | tf_op jit(solution)/shard_map/all_to_all | solution.py:46
  141.2 1.8 broadcast_in_dim.7
  143.0 3.9 all-to-all-start.5
  146.9 1.3 convert_element_type.46
  148.2 1.8 multiply_convert_fusion.1
  150.1 1.3 pad_maximum_fusion
  151.4 25.9 %all-to-all-done.5 = bf16[4,64,1,10,512]{4,1,3,2,0:T(8,128)(2,1)S(1)} async-done(((bf16[4,64,1,10,512]{4,1,3,2,0:T(8,128)(2,1)}), bf16[4,64,1,10,512]{4,1,3,2,0:T(8,128)(2,1)S(1)}, u32[]{:S(2)}, u32[]{:S(2)}) %all-to-all-start.5) | async-done | bytes 2621472 | tf_op jit(solution)/shard_map/all_to_all | solution.py:23
  177.3 7.9 %all-to-all-start = ((bf16[64,32,384]{2,1,0:T(8,128)(2,1)}), bf16[64,32,384]{2,1,0:T(8,128)(2,1)}, u32[]{:S(2)}, u32[]{:S(2)}) async-start(bf16[64,32,384]{2,1,0:T(8,128)(2,1)} %pad_maximum_fusion), calls=%async_computation | async-start | bytes 3145728 | tf_op jit(solution)/shard_map/all_to_all | solution.py:17
  185.2 3.5 copy.93
  188.8 4.3 reshape.84
  193.0 144.8 %all-to-all-done = bf16[64,32,384]{2,1,0:T(8,128)(2,1)} async-done(((bf16[64,32,384]{2,1,0:T(8,128)(2,1)}), bf16[64,32,384]{2,1,0:T(8,128)(2,1)}, u32[]{:S(2)}, u32[]{:S(2)}) %all-to-all-start) | async-done | bytes 1572896 | tf_op jit(solution)/shard_map/all_to_all | solution.py:17
  337.8 2.4 fusion.22
  341.0 8.9 %copy.104 = bf16[1,2048,128]{2,0,1:T(2,128)(2,1)} copy(bf16[1,2048,128]{2,1,0:T(8,128)(2,1)S(1)} %get-tuple-element.4) | data formatting | bytes 1048576 | tf_op jit(solution)/shard_map/split | solution.py:18
  350.5 12.6 %reduce.5 = bf16[2048,128]{1,0:T(8,128)(2,1)S(1)} reduce(bf16[2048,1,128]{2,1,0:T(2,128)(2,1)} %bitcast.61, bf16[]{:T(256)} %broadcast.38), dimensions={1}, to_apply=%bitcast.58.reduce_sub_computation | reduce | bytes 1048578
  363.0 0.9 reshape.94
  363.9 3.8 all-to-all-start.1
  367.7 2.0 fusion.7
  370.5 3.8 all-to-all-done.1
  374.3 1.0 broadcast_in_dim.16
  375.3 3.6 all-to-all-start.6
  378.9 2.2 reshape.95
  382.0 4.5 all-to-all-done.6
  386.5 1.9 convert_bitcast_fusion
  389.0 1.4 copy.95
  390.4 12.6 %all-to-all-start.7 = ((bf16[512,64,10]{0,2,1:T(8,128)(2,1)}), bf16[512,64,10]{0,2,1:T(8,128)(2,1)S(1)}, u32[]{:S(2)}, u32[]{:S(2)}) async-start(bf16[512,64,10]{0,2,1:T(8,128)(2,1)} %copy.95), calls=%async_computation.7 | async-start | bytes 2097152 | tf_op jit(solution)/shard_map/all_to_all | solution.py:125
  403.0 107.4 %all-to-all-done.7 = bf16[512,64,10]{0,2,1:T(8,128)(2,1)S(1)} async-done(((bf16[512,64,10]{0,2,1:T(8,128)(2,1)}), bf16[512,64,10]{0,2,1:T(8,128)(2,1)S(1)}, u32[]{:S(2)}, u32[]{:S(2)}) %all-to-all-start.7) | async-done | bytes 655392 | tf_op jit(solution)/shard_map/all_to_all | solution.py:125
  511.1 1.1 fusion.1
  (39 shorter events, 9.8 us)
Async XLA Ops:
  2.3 9.3 %all-to-all-start.2 = ((f32[4,1,224]{2,1,0:T(1,128)}), f32[4,1,224]{2,1,0:T(1,128)S(1)}, u32[]{:S(2)}, u32[]{:S(2)}) async-start(f32[4,1,224]{2,1,0:T(1,128)} %broadcast_in_dim.6), calls=%async_computation.2 | async-start | bytes 8192 | tf_op jit(solution)/shard_map/all_to_all | solution.py:23
  143.0 5.2 %copy-start.4 = (f32[32]{0:T(128)S(1)}, f32[32]{0:T(128)}, u32[]{:S(2)}) copy-start(f32[32]{0:T(128)} %param.10) | copy-start | bytes 388
  143.0 34.3 %all-to-all-start.5 = ((bf16[4,64,1,10,512]{4,1,3,2,0:T(8,128)(2,1)}), bf16[4,64,1,10,512]{4,1,3,2,0:T(8,128)(2,1)S(1)}, u32[]{:S(2)}, u32[]{:S(2)}) async-start(bf16[4,64,1,10,512]{4,1,3,2,0:T(8,128)(2,1)} %broadcast_in_dim.7), calls=%async_computation.5 | async-start | bytes 5242880 | tf_op jit(solution)/shard_map/all_to_all | solution.py:23
  177.3 160.5 %all-to-all-start = ((bf16[64,32,384]{2,1,0:T(8,128)(2,1)}), bf16[64,32,384]{2,1,0:T(8,128)(2,1)}, u32[]{:S(2)}, u32[]{:S(2)}) async-start(bf16[64,32,384]{2,1,0:T(8,128)(2,1)} %pad_maximum_fusion), calls=%async_computation | async-start | bytes 3145728 | tf_op jit(solution)/shard_map/all_to_all | solution.py:17
  340.2 0.8 copy-start.1
  363.9 10.4 %all-to-all-start.1 = ((bf16[4,2,32768]{2,1,0:T(2,128)(2,1)}), bf16[4,2,32768]{2,1,0:T(2,128)(2,1)S(1)}, u32[]{:S(2)}, u32[]{:S(2)}) async-start(bf16[4,2,32768]{2,1,0:T(2,128)(2,1)} %reshape.94), calls=%async_computation.1 | async-start | bytes 1048576 | tf_op jit(solution)/shard_map/all_to_all | solution.py:113
  367.7 2.0 copy-start.2
  374.3 1.0 copy-start
  375.3 11.1 %all-to-all-start.6 = ((bf16[4,1,64,10,128]{4,2,3,1,0:T(8,128)(2,1)}), bf16[4,1,64,10,128]{4,2,3,1,0:T(8,128)(2,1)S(1)}, u32[]{:S(2)}, u32[]{:S(2)}) async-start(bf16[4,1,64,10,128]{4,2,3,1,0:T(8,128)(2,1)} %broadcast_in_dim.16), calls=%async_computation.6 | async-start | bytes 1310720 | tf_op jit(solution)/shard_map/all_to_all | solution.py:23
  389.0 14.1 %copy-start.3 = (f32[224,2]{0,1:T(2,128)S(1)}, f32[224,2]{0,1:T(2,128)}, u32[]{:S(2)}) copy-start(f32[224,2]{0,1:T(2,128)} %param.9) | copy-start | bytes 5380
  390.4 120.1 %all-to-all-start.7 = ((bf16[512,64,10]{0,2,1:T(8,128)(2,1)}), bf16[512,64,10]{0,2,1:T(8,128)(2,1)S(1)}, u32[]{:S(2)}, u32[]{:S(2)}) async-start(bf16[512,64,10]{0,2,1:T(8,128)(2,1)} %copy.95), calls=%async_computation.7 | async-start | bytes 2097152 | tf_op jit(solution)/shard_map/all_to_all | solution.py:125
where the time goes:
time: 515 us; the launch traced here: 512 us
  waiting for transfers between devices  287 us (56%)
  blocking collectives  126 us (24%)
  starting transfers between devices  36.9 us (7%)
  local copies, waits for them, and re-layouts  32.9 us (6%)
  other arithmetic  20.9 us (4%)
  matrix products  7.59 us (1%)
    all_to_all x1, waiting for transfers between devices, side_by_side(): lax.all_to_all(both, axis, split_axis=split_dim, concat_axis=concat_dim,...  145 us
    all_to_all x2, blocking collectives, exchange_in_order(): filled = lax.all_to_all(filled, axes[k], k, k, tiled=True)  126 us
    all_to_all x1, waiting for transfers between devices, local(): lax.all_to_all(summed.reshape(local_width, shards, per_device * capacity)...  107 us
    all_to_all x3, waiting for transfers between devices, from_everyone(): return lax.all_to_all(copies, axis, split_axis=0, concat_axis=0, tiled=True)  30.9 us
    all_to_all x1, starting transfers between devices, local(): lax.all_to_all(summed.reshape(local_width, shards, per_device * capacity)...  12.6 us
    all_to_all x3, starting transfers between devices, from_everyone(): return lax.all_to_all(copies, axis, split_axis=0, concat_axis=0, tiled=True)  12.6 us
    unnamed x1, other arithmetic  12.6 us
    split x2, local copies, waits for them, and re-layouts, side_by_side(): jnp.split(filled, [sum(widths[:k]) for k in range(1, len(widths))], axis=...  11.3 us
  transfers between devices with their start and end apart: 6, of which 6 were waited for; matrix products, arithmetic and copies ran while one was open for 4% of the time, Pallas kernels for 0%

commit v1 on v0

v1 whole, which is shorter than its diff:
```python
import functools

import jax
import jax.numpy as jnp
from jax import lax
from jax.experimental import pallas as pl
from jax.experimental.pallas import tpu as pltpu
from jax.sharding import PartitionSpec as P

MESH = pl.DeviceIdType.MESH
GRP_FS = ("grp", "fs")
norm_epsilon = 1e-06

LANES = 128
MAIN = 8
TAIL = 2
RANGES = 8
PAIRS = RANGES // 2

f32, bf16 = jnp.float32, jnp.bfloat16


def iota(shape, dim):
    return lax.broadcasted_iota(jnp.int32, shape, dim)


def ones_where(mask):
    return jnp.where(mask, 1.0, 0.0).astype(bf16)


def drain(ref, sem):
    pltpu.make_async_copy(ref, ref, sem).wait()


def dot(a, b, dims=((1,), (0,))):
    return lax.dot_general(a, b, (dims, ((), ())), preferred_element_type=f32)


def flat(tiles):
    n = tiles.shape[0]
    return tiles.astype(f32).reshape(n * MAIN, LANES)


def kernel(
    shards, columns, groups,
    tok, ids, route_w, gain, gate_m, up_m, down_m,
    out_gate, out_up, out_down, out_moe,
    stage, ws, w, wgu, wd, dx, normed, x, gx, lhs, hb, ob, ret, acc, sq, sq_in,
    stage_sem, out_sem, w_send, w_recv, y_send, y_recv, sq_send, sq_recv, d_send, d_recv,
    xf_send, x_recv, dx_send, dx_recv, h_send, h_recv, r_send, r_recv,
):
    S, T, G = shards, columns, groups
    me, tp, grp = lax.axis_index("fs"), lax.axis_index("tp"), lax.axis_index("grp")
    rs = S // RANGES
    rows, width = tok.shape
    chunks = width // LANES
    depth = gate_m.shape[1]
    mine = lax.rem(me, G) == grp

    def fs_peer(r):
        return {"fs": lax.rem(me + r, S)}

    def tp_peer(j):
        return {"tp": lax.rem(tp + j, T)}

    def grp_peer(j):
        return {"grp": lax.rem(grp + j, G)}

    def remote(src, dst, send, recv, peer):
        return pltpu.make_async_remote_copy(
            src_ref=src, dst_ref=dst, send_sem=send, recv_sem=recv, device_id=peer, device_id_type=MESH
        )

    @pl.when(mine)
    def _():
        for a, ref in enumerate((gate_m, up_m, down_m)):
            pltpu.make_async_copy(ref, stage.at[a], stage_sem.at[a]).start()

    barrier = pltpu.get_barrier_semaphore()

    def greet(r, c):
        pl.semaphore_signal(barrier, inc=1, device_id=fs_peer(r), device_id_type=MESH)
        return c

    lax.fori_loop(1, S, greet, 0)
    for j in range(1, T):
        pl.semaphore_signal(barrier, inc=1, device_id=tp_peer(j), device_id_type=MESH)
    for j in range(1, G):
        pl.semaphore_signal(barrier, inc=1, device_id=grp_peer(j), device_id_type=MESH)

    expert_lane = iota((rows, S), 1)
    rel = []
    for k in range(2):
        r = ids[:, k : k + 1] - me
        rel.append(jnp.where(r < 0, r + S, r))
    named = [jnp.where(r == expert_lane, 1.0, 0.0) for r in rel]
    earlier = ones_where(iota((rows, rows), 0) > iota((rows, rows), 1))
    before = dot(earlier, (named[0] + named[1]).astype(bf16))
    diagonal = iota((rows, rows), 0) == iota((rows, rows), 1)
    main, tail, main_row, tail_row = [], [], [], []
    for k in range(2):
        place = jnp.sum(before * named[k], axis=1, keepdims=True)
        base = rel[k].astype(f32) * MAIN
        main.append(jnp.where(place < MAIN, base + place, -1.0))
        tail.append(jnp.where(place < MAIN, -64.0, base + (place - MAIN)))
        main_row.append(jnp.sum(jnp.where(diagonal, main[k], 0.0), axis=0, keepdims=True))
        tail_row.append(jnp.sum(jnp.where(diagonal, tail[k], 0.0), axis=0, keepdims=True))

    values = tok[...].astype(f32)
    squares = jnp.sum(values * values, axis=1, keepdims=True)
    padded = sq.shape[1]
    spread = iota((rows, padded), 0) == iota((rows, padded), 1)
    as_row = jnp.sum(jnp.where(spread, squares, 0.0), axis=0, keepdims=True)
    sq[...] = jnp.broadcast_to(as_row, sq.shape)

    @pl.when(mine)
    def _():
        for a in range(3):
            drain(stage.at[a], stage_sem.at[a])
        eye = iota((depth, depth), 0) == iota((depth, depth), 1)
        column = jnp.sum(jnp.where(eye, gain[...], 0.0), axis=1, keepdims=True)
        scale = jnp.broadcast_to(column, (depth, LANES))

        def convert(r, c):
            e = lax.rem(me + r, S)
            ws[r, 0] = (stage[0, e] * scale).astype(bf16)
            ws[r, 1] = (stage[1, e] * scale).astype(bf16)
            ws[r, 2] = stage[2, e].astype(bf16)
            return c

        lax.fori_loop(0, S, convert, 0)

    pl.semaphore_wait(barrier, (S - 1) + (T - 1) + (G - 1))

    for j in range(1, T):
        remote(sq, sq_in.at[j - 1], sq_send, sq_recv.at[j - 1], tp_peer(j)).start()

    def far_first(i):
        half = (i + 1) // 2
        return S // 2 + half * (2 * lax.rem(i, 2) - 1)

    w_mine = w.at[:, me // G, lax.rem(me, G)]

    @pl.when(mine)
    def _():
        pltpu.make_async_copy(ws.at[0], w_mine, w_recv).start()

        def ship(i, c):
            r = far_first(i)
            remote(ws.at[r], w_mine, w_send, w_recv, fs_peer(r)).start()
            return c

        lax.fori_loop(0, S - 1, ship, 0)

    total = as_row
    for j in range(1, T):
        drain(sq_in.at[j - 1], sq_recv.at[j - 1])
        total = total + sq_in[j - 1][0:1, :]
    squares = jnp.sum(jnp.where(spread, total, 0.0), axis=1, keepdims=True)
    inverse = lax.rsqrt(squares * (1.0 / (width * T)) + norm_epsilon)
    normed[...] = (values * inverse).astype(bf16)
    slot_row = iota((S * MAIN, rows), 0).astype(f32)
    placing = ones_where((slot_row == main_row[0]) | (slot_row == main_row[1]))
    for c in range(chunks):
        y = dot(placing, normed[:, c * LANES : (c + 1) * LANES])
        x[:, c] = y.reshape(S, MAIN, LANES).astype(bf16)
    y = jnp.zeros((S * MAIN, LANES), f32)
    for c in range(chunks):
        here = slot_row - float(TAIL * c)
        placing = ones_where((here == tail_row[0]) | (here == tail_row[1]))
        y = y + dot(placing, normed[:, c * LANES : (c + 1) * LANES])
    x[:, chunks] = y.reshape(S, MAIN, LANES).astype(bf16)

    pltpu.make_async_copy(x.at[0], gx.at[tp, 0], d_recv.at[0]).start()

    def dispatch(i, c):
        r = far_first(i)
        d = S - r
        remote(x.at[r], gx.at[tp, d], d_send, d_recv.at[d // rs], fs_peer(r)).start()
        return c

    lax.fori_loop(0, S - 1, dispatch, 0)

    def ranges_of(p):
        return (PAIRS - 1 - p, PAIRS + p)

    def forward(p):
        for q in ranges_of(p):
            part = pl.ds(q * rs, rs)
            drain(gx.at[tp, part], d_recv.at[q])
            for j in range(1, T):
                remote(gx.at[tp, part], gx.at[tp, part], xf_send, x_recv.at[p], tp_peer(j)).start()

    drain(w.at[:, :, grp], w_recv)
    for j in range(1, G):
        remote(w.at[:, :, grp], w.at[:, :, grp], y_send, y_recv.at[j - 1], grp_peer(j)).start()
    forward(0)
    for j in range(1, G):
        drain(w.at[:, :, lax.rem(grp + G - j, G)], y_recv.at[j - 1])
    strip = S // T // G
    pltpu.make_async_copy(w.at[2, pl.ds(tp * strip, strip)], dx.at[tp], dx_recv).start()
    for j in range(1, T):
        there = lax.rem(tp + j, T)
        remote(w.at[2, pl.ds(there * strip, strip)], dx.at[tp], dx_send, dx_recv, tp_peer(j)).start()
    outs = (out_gate, out_up, out_down)
    for a, ref in enumerate(outs):
        pltpu.make_async_copy(w.at[a], ref, out_sem.at[a]).start()
    wgu[:, :LANES] = w[0].reshape(S * depth, LANES)
    wgu[:, LANES:] = w[1].reshape(S * depth, LANES)
    drain(dx, dx_recv)
    for j in range(T):
        wd[:, j * LANES : (j + 1) * LANES] = dx[j].reshape(width, LANES)

    half = rs * MAIN
    n_main, n_tail = 2 * half, 2 * rs * TAIL
    q_of = iota((n_tail, n_main), 0)
    tail_home = (q_of >> 1) * MAIN + (q_of & 1)
    picks = [ones_where(iota((n_tail, n_main), 1) == tail_home + TAIL * c) for c in range(chunks)]
    q_of = iota((n_main, n_tail), 1)
    tail_home = (q_of >> 1) * MAIN + (q_of & 1)
    puts = [ones_where(iota((n_main, n_tail), 0) == tail_home + TAIL * c) for c in range(chunks)]

    def first_half(p):
        drain(gx.at[pl.ds(0, T - 1), pl.ds(0, 2 * rs)], x_recv.at[p])
        for j in range(T):
            for s, q in enumerate(ranges_of(p)):
                part = slice(q * rs, (q + 1) * rs)
                for c in range(chunks):
                    k = j * chunks + c
                    lhs[s * half : (s + 1) * half, k * LANES : (k + 1) * LANES] = flat(gx[j, part, c]).astype(bf16)
            tails = jnp.concatenate(
                [flat(gx[j, q * rs : (q + 1) * rs, chunks]) for q in ranges_of(p)], axis=0
            ).astype(bf16)
            for c in range(chunks):
                k = j * chunks + c
                lhs[n_main:, k * LANES : (k + 1) * LANES] = dot(picks[c], tails).astype(bf16)
        both = dot(lhs[...], wgu[...])
        gate, up = both[:, :LANES], both[:, LANES:]
        hb[p, tp] = (gate / (1.0 + jnp.exp(-gate)) * up).astype(bf16)
        for j in range(1, T):
            remote(hb.at[p, tp], hb.at[p, tp], h_send, h_recv.at[p], tp_peer(j)).start()

    def send_back(d):
        back = lax.rem(S - d, S)
        remote(ob.at[d], ret.at[back], r_send, r_recv.at[back // rs], fs_peer(d)).start()

    def second_half(p):
        drain(hb.at[p, pl.ds(0, T - 1)], h_recv.at[p])
        hidden = jnp.concatenate([hb[p, j] for j in range(T)], axis=1)
        o = dot(hidden, wd[...], ((1,), (1,)))
        y = jnp.zeros((n_main, LANES), f32)
        for c in range(chunks):
            lanes = slice(c * LANES, (c + 1) * LANES)
            y = y + dot(puts[c], o[n_main:, lanes].astype(bf16))
        for s, q in enumerate(ranges_of(p)):
            part = slice(q * rs, (q + 1) * rs)
            for c in range(chunks):
                lanes = slice(c * LANES, (c + 1) * LANES)
                ob[part, c] = o[s * half : (s + 1) * half, lanes].reshape(rs, MAIN, LANES).astype(bf16)
            ob[part, chunks] = y[s * half : (s + 1) * half].reshape(rs, MAIN, LANES).astype(bf16)
        near, far = ranges_of(p)

        def send(i, c):
            send_back(far * rs + i)
            send_back(near * rs + rs - 1 - i)
            return c

        if near:
            lax.fori_loop(0, rs, send, 0)
        else:
            lax.fori_loop(0, rs - 1, send, 0)
            send_back(far * rs + rs - 1)
            pltpu.make_async_copy(ob.at[0], ret.at[0], r_recv.at[0]).start()

    for p in range(PAIRS):
        first_half(p)
        if p + 1 < PAIRS:
            forward(p + 1)
        second_half(p)

    acc[...] = jnp.zeros_like(acc)
    for p in range(PAIRS):
        near, far = ranges_of(p)
        lane = iota((rows, n_main), 1)
        home = jnp.where(lane < half, lane + near * half, lane + (far - 1) * half).astype(f32)
        for q in (near, far):
            drain(ret.at[pl.ds(q * rs, rs)], r_recv.at[q])

        def piece(c):
            return jnp.concatenate(
                [flat(ret[q * rs : (q + 1) * rs, c]) for q in (near, far)], axis=0
            ).astype(bf16)

        tails = piece(chunks)
        for c in range(chunks):
            lanes = slice(c * LANES, (c + 1) * LANES)
            values = piece(c)
            for k in range(2):
                acc[k, :, lanes] += dot(ones_where(home == main[k]), values) + dot(
                    ones_where(home == tail[k] + float(TAIL * c)), tails
                )
    out_moe[...] = (route_w[:, 0:1] * acc[0] + route_w[:, 1:2] * acc[1]).astype(bf16)

    drain(sq_in, sq_send)

    @pl.when(mine)
    def _():
        drain(ws.at[pl.ds(1, S - 1)], w_send)

    drain(x.at[pl.ds(1, S - 1)], d_send)
    drain(w.at[:, :, pl.ds(0, G - 1)], y_send)
    drain(gx.at[pl.ds(0, T - 1)], xf_send)
    drain(dx.at[pl.ds(0, T - 1)], dx_send)
    drain(hb.at[:, pl.ds(0, T - 1)], h_send)
    drain(ob.at[pl.ds(1, S - 1)], r_send)
    for a, ref in enumerate(outs):
        drain(w.at[a], out_sem.at[a])


def local(shards, columns, groups, tokens, route_ids, route_weights, norm_gain, gate_m, up_m, down_m):
    S, T, G = shards, columns, groups
    rows, width = tokens.shape
    depth = gate_m.shape[1]
    chunks = width // LANES
    rs = S // RANGES
    padded = -(-rows // LANES) * LANES
    n_rows = 2 * rs * (MAIN + TAIL)
    vmem = pl.BlockSpec(memory_space=pltpu.VMEM)
    anywhere = pl.BlockSpec(memory_space=pl.ANY)
    dma = pltpu.SemaphoreType.DMA
    block = (chunks + 1, MAIN, LANES)
    served = jax.ShapeDtypeStruct((S // G, G, depth, LANES), bf16)
    outs = pl.pallas_call(
        functools.partial(kernel, S, T, G),
        out_shape=(served, served, served, jax.ShapeDtypeStruct((rows, width), bf16)),
        in_specs=[vmem] * 4 + [anywhere] * 3,
        out_specs=(anywhere, anywhere, anywhere, vmem),
        scratch_shapes=[
            pltpu.VMEM((3, S, depth, LANES), f32),
            pltpu.VMEM((S, 3, depth, LANES), bf16),
            pltpu.VMEM((3, S // G, G, depth, LANES), bf16),
            pltpu.VMEM((S * depth, 2 * LANES), bf16),
            pltpu.VMEM((width, T * LANES), bf16),
            pltpu.VMEM((T, S // T // G, G, depth, LANES), bf16),
            pltpu.VMEM((rows, width), bf16),
            pltpu.VMEM((S, *block), bf16),
            pltpu.VMEM((T, S, *block), bf16),
            pltpu.VMEM((n_rows, T * width), bf16),
            pltpu.VMEM((PAIRS, T, n_rows, LANES), bf16),
            pltpu.VMEM((S, *block), bf16),
            pltpu.VMEM((S, *block), bf16),
            pltpu.VMEM((2, rows, width), f32),
            pltpu.VMEM((MAIN, padded), f32),
            pltpu.VMEM((T - 1, MAIN, padded), f32),
            dma((3,)), dma((3,)), dma, dma, dma, dma((max(G - 1, 1),)), dma, dma((T - 1,)), dma, dma((RANGES,)),
            dma, dma((PAIRS,)), dma, dma, dma, dma((PAIRS,)), dma, dma((RANGES,)),
        ],
        compiler_params=pltpu.CompilerParams(collective_id=0, has_side_effects=True),
    )(tokens, route_ids, route_weights, norm_gain[None, :], gate_m, up_m, down_m)
    gate, up, down = (o.reshape(1, S * depth, LANES) for o in outs[:3])
    return gate, up, down, outs[3]


def solution(mesh):
    placed = (
        P(GRP_FS, "tp"), P(GRP_FS, None), P(GRP_FS, None), P("fs"),
        P(None, "fs", "tp"), P(None, "fs", "tp"), P(None, "fs", "tp"),
    )
    return jax.shard_map(
        functools.partial(local, mesh.shape["fs"], mesh.shape["tp"], mesh.shape["grp"]),
        mesh=mesh,
        in_specs=placed,
        out_specs=(P(GRP_FS, None, "tp"), P(GRP_FS, None, "tp"), P(GRP_FS, None, "tp"), P(GRP_FS, "tp")),
        check_vma=False,
    )
```

time: 515 us -> 262 us (0.51)
  waiting for transfers between devices: 287 us -> 0 us
  Pallas kernels: 0 us -> 253 us
  blocking collectives: 126 us -> 0 us
  starting transfers between devices: 36.9 us -> 0 us
  local copies, waits for them, and re-layouts: 32.9 us -> 7.22 us
  other arithmetic: 20.9 us -> 0 us
  matrix products: 7.59 us -> 0 us
    all_to_all x6 -> x0, waiting for transfers between devices: 287 us -> none  [the longest x1 145 us: side_by_side(): lax.all_to_all(both, axis, split_axis=split_dim, concat_axis=concat_dim,...]
    pallas_call x0 -> x1, Pallas kernels: none -> 253 us  [local(): pl.pallas_call(functools.partial(kernel, S, T, G), out_shape=(served, ser...]
    all_to_all x2 -> x0, blocking collectives: 126 us -> none  [exchange_in_order(): filled = lax.all_to_all(filled, axes[k], k, k, tiled=True)]
    all_to_all x6 -> x0, starting transfers between devices: 36.9 us -> none  [the longest x1 12.6 us: local(): lax.all_to_all(summed.reshape(local_width, shards, per_device * capacity)...]
    unnamed x1 -> x0, other arithmetic: 12.6 us -> none
    split x2 -> x0, local copies, waits for them, and re-layouts: 11.3 us -> none  [side_by_side(): jnp.split(filled, [sum(widths[:k]) for k in range(1, len(widths))], axis=...]
    dot_general x6 -> x0, matrix products: 7.59 us -> none  [the longest x1 1.95 us: local(): jnp.einsum('sxcd,xdf->xscf', partial_value, gate_serve, preferred_element...]
  transfers between devices with their start and end apart: 6 -> 0, of which waited for: 6 -> 0; matrix products, arithmetic and copies ran while one was open for 4% -> 0% of each run, Pallas kernels for 0% -> 0%
where the time goes in v1:
time: 262 us; the launch traced here: 261 us
  Pallas kernels  253 us (97%)
  local copies, waits for them, and re-layouts  7.22 us (3%)
    pallas_call x1, Pallas kernels, local(): pl.pallas_call(functools.partial(kernel, S, T, G), out_shape=(served, ser...  253 us
    unnamed x14, local copies, waits for them, and re-layouts  7.22 us

profile of v1, /device:TPU:33, one launch (start us, length us, event | category | flops | bytes accessed | tf_op | source)
XLA Modules:
  0.0 260.6 jit_solution(15978016493375212460)
XLA Ops:
  0.6 0.0 copy-start.3
  0.6 1.5 copy.11.ids
  2.1 0.0 copy-done.3
  2.1 0.8 copy.12.route_w
  2.9 252.7 %shard_map.102 = (bf16[32,2,32,128]{3,2,1,0:T(8,128)(2,1)}, bf16[32,2,32,128]{3,2,1,0:T(8,128)(2,1)}, bf16[32,2,32,128]{3,2,1,0:T(8,128)(2,1)}, bf16[224,512]{1,0:T(8,128)(2,1)}) custom-call(bf16[224,512]{1,0:T(8,128)(2,1)} %tok.1, s32[224,2]{1,0:T(8,128)} %copy.11.ids, f32[224,2]{1,0:T(8,128)} %copy.12.route_w, f32[1,32]{1,0:T(1,128)} %bitcast.7, ...), custom_call_target="tpu_custom_call" | custom-call | tf_op jit(solution)/shard_map/pallas_call | solution.py:333
  255.6 0.0 copy-start.1
  255.7 1.9 copy.17
  257.6 0.0 copy-done.1
  257.6 0.0 copy-start
  257.6 0.8 copy.18
  258.4 0.4 copy-done
  258.8 0.0 copy-start.2
  258.8 0.8 copy.19
  259.6 0.3 copy-done.2
  259.9 0.7 copy.20
Async XLA Ops:
  0.6 1.5 copy-start.3
  255.6 1.9 copy-start.1
  257.6 1.2 copy-start
  258.8 1.1 copy-start.2

commit v2 on v1

--- a/solution.py
+++ b/solution.py
@@ -45,7 +45,7 @@
     shards, columns, groups,
     tok, ids, route_w, gain, gate_m, up_m, down_m,
     out_gate, out_up, out_down, out_moe,
-    stage, ws, w, wgu, wd, dx, normed, x, gx, lhs, hb, ob, ret, acc, sq, sq_in,
+    stage, ws, w, wgu, wd, dx, normed, x, gx, lhs, hb, ob, ret, acc, sq, sq_in, ready,
     stage_sem, out_sem, w_send, w_recv, y_send, y_recv, sq_send, sq_recv, d_send, d_recv,
     xf_send, x_recv, dx_send, dx_recv, h_send, h_recv, r_send, r_recv,
 ):
@@ -76,17 +76,58 @@
         for a, ref in enumerate((gate_m, up_m, down_m)):
             pltpu.make_async_copy(ref, stage.at[a], stage_sem.at[a]).start()
 
+    place_of = lax.rem(me + S - 1, S)
+
+    def placed_at(q):
+        return {"fs": lax.rem(q + 1, S)}
+
     barrier = pltpu.get_barrier_semaphore()
-
-    def greet(r, c):
-        pl.semaphore_signal(barrier, inc=1, device_id=fs_peer(r), device_id_type=MESH)
-        return c
-
-    lax.fori_loop(1, S, greet, 0)
     for j in range(1, T):
         pl.semaphore_signal(barrier, inc=1, device_id=tp_peer(j), device_id_type=MESH)
     for j in range(1, G):
         pl.semaphore_signal(barrier, inc=1, device_id=grp_peer(j), device_id_type=MESH)
+    pl.semaphore_wait(barrier, (T - 1) + (G - 1) + (place_of + S - 1) // S)
+
+    @pl.when(place_of < S - 1)
+    def _():
+        pl.semaphore_signal(barrier, inc=1, device_id=placed_at(place_of + 1), device_id_type=MESH)
+
+    def report(q, c):
+        pl.semaphore_signal(ready.at[place_of], inc=1, device_id=placed_at(q), device_id_type=MESH)
+        return c
+
+    lax.fori_loop(0, place_of, report, 0)
+
+    w_mine = w.at[:, me // G, lax.rem(me, G)]
+
+    def ship(q):
+        r = lax.rem(q + 1 + S - me, S)
+        remote(ws.at[r], w_mine, w_send, w_recv, placed_at(q)).start()
+
+    @pl.when(mine)
+    def _():
+        for a in range(3):
+            drain(stage.at[a], stage_sem.at[a])
+        eye = iota((depth, depth), 0) == iota((depth, depth), 1)
+        column = jnp.sum(jnp.where(eye, gain[...], 0.0), axis=1, keepdims=True)
+        scale = jnp.broadcast_to(column, (depth, LANES))
+
+        def convert(r, c):
+            e = lax.rem(me + r, S)
+            ws[r, 0] = (stage[0, e] * scale).astype(bf16)
+            ws[r, 1] = (stage[1, e] * scale).astype(bf16)
+            ws[r, 2] = stage[2, e].astype(bf16)
+            return c
+
+        lax.fori_loop(0, S, convert, 0)
+        pltpu.make_async_copy(ws.at[0], w_mine, w_recv).start()
+
+        def ship_before(i, c):
+            odd = lax.rem(i, 2)
+            ship(odd * (i // 2) + (1 - odd) * (place_of - 1 - i // 2))
+            return c
+
+        lax.fori_loop(0, place_of, ship_before, 0)
 
     expert_lane = iota((rows, S), 1)
     rel = []
@@ -113,44 +154,12 @@
     as_row = jnp.sum(jnp.where(spread, squares, 0.0), axis=0, keepdims=True)
     sq[...] = jnp.broadcast_to(as_row, sq.shape)
 
-    @pl.when(mine)
-    def _():
-        for a in range(3):
-            drain(stage.at[a], stage_sem.at[a])
-        eye = iota((depth, depth), 0) == iota((depth, depth), 1)
-        column = jnp.sum(jnp.where(eye, gain[...], 0.0), axis=1, keepdims=True)
-        scale = jnp.broadcast_to(column, (depth, LANES))
-
-        def convert(r, c):
-            e = lax.rem(me + r, S)
-            ws[r, 0] = (stage[0, e] * scale).astype(bf16)
-            ws[r, 1] = (stage[1, e] * scale).astype(bf16)
-            ws[r, 2] = stage[2, e].astype(bf16)
-            return c
-
-        lax.fori_loop(0, S, convert, 0)
-
-    pl.semaphore_wait(barrier, (S - 1) + (T - 1) + (G - 1))
-
     for j in range(1, T):
         remote(sq, sq_in.at[j - 1], sq_send, sq_recv.at[j - 1], tp_peer(j)).start()
 
     def far_first(i):
         half = (i + 1) // 2
         return S // 2 + half * (2 * lax.rem(i, 2) - 1)
-
-    w_mine = w.at[:, me // G, lax.rem(me, G)]
-
-    @pl.when(mine)
-    def _():
-        pltpu.make_async_copy(ws.at[0], w_mine, w_recv).start()
-
-        def ship(i, c):
-            r = far_first(i)
-            remote(ws.at[r], w_mine, w_send, w_recv, fs_peer(r)).start()
-            return c
-
-        lax.fori_loop(0, S - 1, ship, 0)
 
     total = as_row
     for j in range(1, T):
@@ -170,6 +179,17 @@
         placing = ones_where((here == tail_row[0]) | (here == tail_row[1]))
         y = y + dot(placing, normed[:, c * LANES : (c + 1) * LANES])
     x[:, chunks] = y.reshape(S, MAIN, LANES).astype(bf16)
+
+    def ship_after(q, c):
+        pl.semaphore_wait(ready.at[q], 1)
+
+        @pl.when(mine)
+        def _():
+            ship(q)
+
+        return c
+
+    lax.fori_loop(place_of + 1, S, ship_after, 0)
 
     pltpu.make_async_copy(x.at[0], gx.at[tp, 0], d_recv.at[0]).start()
 
@@ -352,6 +372,7 @@
             pltpu.VMEM((2, rows, width), f32),
             pltpu.VMEM((MAIN, padded), f32),
             pltpu.VMEM((T - 1, MAIN, padded), f32),
+            pltpu.SemaphoreType.REGULAR((S,)),
             dma((3,)), dma((3,)), dma, dma, dma, dma((max(G - 1, 1),)), dma, dma((T - 1,)), dma, dma((RANGES,)),
             dma, dma((PAIRS,)), dma, dma, dma, dma((PAIRS,)), dma, dma((RANGES,)),
         ],

time: 262 us -> 258 us (0.985)
  Pallas kernels: 253 us -> 250 us
    pallas_call x1, Pallas kernels: 253 us -> 250 us  [local(): pl.pallas_call(functools.partial(kernel, S, T, G), out_shape=(served, ser...]
where the time goes in v2:
time: 258 us
  Pallas kernels  250 us (97%)
  local copies, waits for them, and re-layouts  7.22 us (3%)
    pallas_call x1, Pallas kernels, local(): pl.pallas_call(functools.partial(kernel, S, T, G), out_shape=(served, ser...  250 us
    unnamed x14, local copies, waits for them, and re-layouts  7.22 us

profile of v2, /device:TPU:33, one launch (start us, length us, event | category | flops | bytes accessed | tf_op | source)
XLA Modules:
  0.0 257.9 jit_solution(477902480845481048)
XLA Ops:
  0.6 0.0 copy-start.3
  0.6 1.5 copy.11.ids
  2.1 0.0 copy-done.3
  2.1 0.8 copy.12.route_w
  2.9 250.0 %shard_map.102 = (bf16[32,2,32,128]{3,2,1,0:T(8,128)(2,1)}, bf16[32,2,32,128]{3,2,1,0:T(8,128)(2,1)}, bf16[32,2,32,128]{3,2,1,0:T(8,128)(2,1)}, bf16[224,512]{1,0:T(8,128)(2,1)}) custom-call(bf16[224,512]{1,0:T(8,128)(2,1)} %tok.1, s32[224,2]{1,0:T(8,128)} %copy.11.ids, f32[224,2]{1,0:T(8,128)} %copy.12.route_w, f32[1,32]{1,0:T(1,128)} %bitcast.7, ...), custom_call_target="tpu_custom_call" | custom-call | tf_op jit(solution)/shard_map/pallas_call | solution.py:353
  252.9 0.0 copy-start.1
  252.9 1.9 copy.17
  254.8 0.0 copy-done.1
  254.8 0.0 copy-start
  254.8 0.8 copy.18
  255.6 0.4 copy-done
  256.0 0.0 copy-start.2
  256.0 0.8 copy.19
  256.8 0.3 copy-done.2
  257.2 0.7 copy.20
Async XLA Ops:
  0.6 1.5 copy-start.3
  252.9 1.9 copy-start.1
  254.8 1.2 copy-start
  256.0 1.1 copy-start.2

commit v3 on v2

--- a/solution.py
+++ b/solution.py
@@ -82,15 +82,17 @@
         return {"fs": lax.rem(q + 1, S)}
 
     barrier = pltpu.get_barrier_semaphore()
+
+    def greet(q, c):
+        pl.semaphore_signal(barrier, inc=1, device_id=placed_at(q), device_id_type=MESH)
+        return c
+
+    lax.fori_loop(place_of + 1, S, greet, 0)
     for j in range(1, T):
         pl.semaphore_signal(barrier, inc=1, device_id=tp_peer(j), device_id_type=MESH)
     for j in range(1, G):
         pl.semaphore_signal(barrier, inc=1, device_id=grp_peer(j), device_id_type=MESH)
-    pl.semaphore_wait(barrier, (T - 1) + (G - 1) + (place_of + S - 1) // S)
-
-    @pl.when(place_of < S - 1)
-    def _():
-        pl.semaphore_signal(barrier, inc=1, device_id=placed_at(place_of + 1), device_id_type=MESH)
+    pl.semaphore_wait(barrier, place_of + (T - 1) + (G - 1))
 
     def report(q, c):
         pl.semaphore_signal(ready.at[place_of], inc=1, device_id=placed_at(q), device_id_type=MESH)
@@ -129,19 +131,23 @@
 
         lax.fori_loop(0, place_of, ship_before, 0)
 
-    expert_lane = iota((rows, S), 1)
+    diagonal = iota((rows, rows), 0) == iota((rows, rows), 1)
+
+    def as_column(row):
+        return jnp.sum(jnp.where(diagonal, row, 0.0), axis=1, keepdims=True)
+
+    expert_lane = iota((rows, S), 1).astype(f32)
     rel = []
     for k in range(2):
-        r = ids[:, k : k + 1] - me
-        rel.append(jnp.where(r < 0, r + S, r))
+        r = ids[k : k + 1, :] - me
+        rel.append(as_column(jnp.where(r < 0, r + S, r).astype(f32)))
     named = [jnp.where(r == expert_lane, 1.0, 0.0) for r in rel]
     earlier = ones_where(iota((rows, rows), 0) > iota((rows, rows), 1))
     before = dot(earlier, (named[0] + named[1]).astype(bf16))
-    diagonal = iota((rows, rows), 0) == iota((rows, rows), 1)
     main, tail, main_row, tail_row = [], [], [], []
     for k in range(2):
         place = jnp.sum(before * named[k], axis=1, keepdims=True)
-        base = rel[k].astype(f32) * MAIN
+        base = rel[k] * MAIN
         main.append(jnp.where(place < MAIN, base + place, -1.0))
         tail.append(jnp.where(place < MAIN, -64.0, base + (place - MAIN)))
         main_row.append(jnp.sum(jnp.where(diagonal, main[k], 0.0), axis=0, keepdims=True))
@@ -319,7 +325,8 @@
                 acc[k, :, lanes] += dot(ones_where(home == main[k]), values) + dot(
                     ones_where(home == tail[k] + float(TAIL * c)), tails
                 )
-    out_moe[...] = (route_w[:, 0:1] * acc[0] + route_w[:, 1:2] * acc[1]).astype(bf16)
+    weight = [as_column(route_w[k : k + 1, :]) for k in range(2)]
+    out_moe[...] = (weight[0] * acc[0] + weight[1] * acc[1]).astype(bf16)
 
     drain(sq_in, sq_send)
 
@@ -377,7 +384,7 @@
             dma, dma((PAIRS,)), dma, dma, dma, dma((PAIRS,)), dma, dma((RANGES,)),
         ],
         compiler_params=pltpu.CompilerParams(collective_id=0, has_side_effects=True),
-    )(tokens, route_ids, route_weights, norm_gain[None, :], gate_m, up_m, down_m)
+    )(tokens, route_ids.T, route_weights.T, norm_gain[None, :], gate_m, up_m, down_m)
     gate, up, down = (o.reshape(1, S * depth, LANES) for o in outs[:3])
     return gate, up, down, outs[3]
 

time: 258 us -> 256 us (level)
    unnamed x14 -> x10, local copies, waits for them, and re-layouts: 7.22 us -> 4.97 us
where the time goes in v3:
time: 256 us; the launch traced here: 255 us
  Pallas kernels  250 us (98%)
  local copies, waits for them, and re-layouts  4.97 us (2%)
    pallas_call x1, Pallas kernels, local(): pl.pallas_call(functools.partial(kernel, S, T, G), out_shape=(served, ser...  250 us

profile of v3, /device:TPU:33, one launch (start us, length us, event | category | flops | bytes accessed | tf_op | source)
XLA Modules:
  0.0 255.4 jit_solution(14763074350592970815)
XLA Ops:
  0.6 249.8 %shard_map.102 = (bf16[32,2,32,128]{3,2,1,0:T(8,128)(2,1)}, bf16[32,2,32,128]{3,2,1,0:T(8,128)(2,1)}, bf16[32,2,32,128]{3,2,1,0:T(8,128)(2,1)}, bf16[224,512]{1,0:T(8,128)(2,1)}) custom-call(bf16[224,512]{1,0:T(8,128)(2,1)} %tok.1, s32[2,224]{1,0:T(2,128)} %bitcast.9, f32[2,224]{1,0:T(2,128)} %bitcast.10, f32[1,32]{1,0:T(1,128)} %bitcast.11, ...), custom_call_target="tpu_custom_call" | custom-call | tf_op jit(solution)/shard_map/pallas_call | solution.py:360
  250.4 0.0 copy-start.1
  250.4 1.9 copy.15
  252.3 0.0 copy-done.1
  252.3 0.0 copy-start
  252.3 0.8 copy.16
  253.1 0.4 copy-done
  253.6 0.0 copy-start.2
  253.6 0.8 copy.17
  254.4 0.3 copy-done.2
  254.7 0.7 copy.18
Async XLA Ops:
  250.4 1.9 copy-start.1
  252.3 1.2 copy-start
  253.6 1.1 copy-start.2

commit v4 on v3

--- a/solution.py
+++ b/solution.py
@@ -30,6 +30,17 @@
 
 def drain(ref, sem):
     pltpu.make_async_copy(ref, ref, sem).wait()
+
+
+def parts_of(groups):
+    rows = min(groups, 4)
+    return groups // rows, rows
+
+
+def tall(blocks):
+    if blocks.shape[-2] % 16:
+        return blocks.astype(f32).reshape(-1, LANES).astype(bf16)
+    return blocks.reshape(-1, LANES)
 
 
 def dot(a, b, dims=((1,), (0,))):
@@ -55,7 +66,10 @@
     rows, width = tok.shape
     chunks = width // LANES
     depth = gate_m.shape[1]
-    mine = lax.rem(me, G) == grp
+    Q, R = parts_of(G)
+    strip = depth // R
+    turn, part = grp // R, lax.rem(grp, R)
+    mine = lax.rem(me, Q) == turn
 
     def fs_peer(r):
         return {"fs": lax.rem(me + r, S)}
@@ -74,7 +88,7 @@
     @pl.when(mine)
     def _():
         for a, ref in enumerate((gate_m, up_m, down_m)):
-            pltpu.make_async_copy(ref, stage.at[a], stage_sem.at[a]).start()
+            pltpu.make_async_copy(ref.at[:, pl.ds(part * strip, strip)], stage.at[a], stage_sem.at[a]).start()
 
     place_of = lax.rem(me + S - 1, S)
 
@@ -100,7 +114,8 @@
 
     lax.fori_loop(0, place_of, report, 0)
 
-    w_mine = w.at[:, me // G, lax.rem(me, G)]
+    w_mine = w.at[:, me // Q, lax.rem(me, Q), part]
+    w_group = w.at[:, :, turn, part]
 
     def ship(q):
         r = lax.rem(q + 1 + S - me, S)
@@ -110,9 +125,9 @@
     def _():
         for a in range(3):
             drain(stage.at[a], stage_sem.at[a])
-        eye = iota((depth, depth), 0) == iota((depth, depth), 1)
+        eye = iota((strip, depth), 0) + part * strip == iota((strip, depth), 1)
         column = jnp.sum(jnp.where(eye, gain[...], 0.0), axis=1, keepdims=True)
-        scale = jnp.broadcast_to(column, (depth, LANES))
+        scale = jnp.broadcast_to(column, (strip, LANES))
 
         def convert(r, c):
             e = lax.rem(me + r, S)
@@ -217,25 +232,26 @@
             for j in range(1, T):
                 remote(gx.at[tp, part], gx.at[tp, part], xf_send, x_recv.at[p], tp_peer(j)).start()
 
-    drain(w.at[:, :, grp], w_recv)
+    drain(w_group, w_recv)
     for j in range(1, G):
-        remote(w.at[:, :, grp], w.at[:, :, grp], y_send, y_recv.at[j - 1], grp_peer(j)).start()
+        remote(w_group, w_group, y_send, y_recv.at[j - 1], grp_peer(j)).start()
     forward(0)
     for j in range(1, G):
-        drain(w.at[:, :, lax.rem(grp + G - j, G)], y_recv.at[j - 1])
-    strip = S // T // G
-    pltpu.make_async_copy(w.at[2, pl.ds(tp * strip, strip)], dx.at[tp], dx_recv).start()
+        other = lax.rem(grp + G - j, G)
+        drain(w.at[:, :, other // R, lax.rem(other, R)], y_recv.at[j - 1])
+    share = S // T // Q
+    pltpu.make_async_copy(w.at[2, pl.ds(tp * share, share)], dx.at[tp], dx_recv).start()
     for j in range(1, T):
         there = lax.rem(tp + j, T)
-        remote(w.at[2, pl.ds(there * strip, strip)], dx.at[tp], dx_send, dx_recv, tp_peer(j)).start()
+        remote(w.at[2, pl.ds(there * share, share)], dx.at[tp], dx_send, dx_recv, tp_peer(j)).start()
     outs = (out_gate, out_up, out_down)
     for a, ref in enumerate(outs):
         pltpu.make_async_copy(w.at[a], ref, out_sem.at[a]).start()
-    wgu[:, :LANES] = w[0].reshape(S * depth, LANES)
-    wgu[:, LANES:] = w[1].reshape(S * depth, LANES)
+    wgu[:, :LANES] = tall(w[0])
+    wgu[:, LANES:] = tall(w[1])
     drain(dx, dx_recv)
     for j in range(T):
-        wd[:, j * LANES : (j + 1) * LANES] = dx[j].reshape(width, LANES)
+        wd[:, j * LANES : (j + 1) * LANES] = tall(dx[j])
 
     half = rs * MAIN
     n_main, n_tail = 2 * half, 2 * rs * TAIL
@@ -335,7 +351,8 @@
         drain(ws.at[pl.ds(1, S - 1)], w_send)
 
     drain(x.at[pl.ds(1, S - 1)], d_send)
-    drain(w.at[:, :, pl.ds(0, G - 1)], y_send)
+    for j in range(1, G):
+        drain(w_group, y_send)
     drain(gx.at[pl.ds(0, T - 1)], xf_send)
     drain(dx.at[pl.ds(0, T - 1)], dx_send)
     drain(hb.at[:, pl.ds(0, T - 1)], h_send)
@@ -356,19 +373,21 @@
     anywhere = pl.BlockSpec(memory_space=pl.ANY)
     dma = pltpu.SemaphoreType.DMA
     block = (chunks + 1, MAIN, LANES)
-    served = jax.ShapeDtypeStruct((S // G, G, depth, LANES), bf16)
+    Q, R = parts_of(G)
+    strip = depth // R
+    served = jax.ShapeDtypeStruct((S // Q, Q, R, strip, LANES), bf16)
     outs = pl.pallas_call(
         functools.partial(kernel, S, T, G),
         out_shape=(served, served, served, jax.ShapeDtypeStruct((rows, width), bf16)),
         in_specs=[vmem] * 4 + [anywhere] * 3,
         out_specs=(anywhere, anywhere, anywhere, vmem),
         scratch_shapes=[
-            pltpu.VMEM((3, S, depth, LANES), f32),
-            pltpu.VMEM((S, 3, depth, LANES), bf16),
-            pltpu.VMEM((3, S // G, G, depth, LANES), bf16),
+            pltpu.VMEM((3, S, strip, LANES), f32),
+            pltpu.VMEM((S, 3, strip, LANES), bf16),
+            pltpu.VMEM((3, S // Q, Q, R, strip, LANES), bf16),
             pltpu.VMEM((S * depth, 2 * LANES), bf16),
             pltpu.VMEM((width, T * LANES), bf16),
-            pltpu.VMEM((T, S // T // G, G, depth, LANES), bf16),
+            pltpu.VMEM((T, S // T // Q, Q, R, strip, LANES), bf16),
             pltpu.VMEM((rows, width), bf16),
             pltpu.VMEM((S, *block), bf16),
             pltpu.VMEM((T, S, *block), bf16),

time: 256 us -> 244 us (0.953)
  Pallas kernels: 250 us -> 238 us
    pallas_call x1, Pallas kernels: 250 us -> 238 us  [local(): pl.pallas_call(functools.partial(kernel, S, T, G), out_shape=(served, ser...]
where the time goes in v4:
time: 244 us
  Pallas kernels  238 us (98%)
  local copies, waits for them, and re-layouts  4.97 us (2%)
    pallas_call x1, Pallas kernels, local(): pl.pallas_call(functools.partial(kernel, S, T, G), out_shape=(served, ser...  238 us
    unnamed x10, local copies, waits for them, and re-layouts  4.97 us

profile of v4, /device:TPU:33, one launch (start us, length us, event | category | flops | bytes accessed | tf_op | source)
XLA Modules:
  0.0 243.6 jit_solution(15976742020365741464)
XLA Ops:
  0.6 238.0 %shard_map.102 = (bf16[64,1,2,16,128]{4,3,2,1,0:T(8,128)(2,1)}, bf16[64,1,2,16,128]{4,3,2,1,0:T(8,128)(2,1)}, bf16[64,1,2,16,128]{4,3,2,1,0:T(8,128)(2,1)}, bf16[224,512]{1,0:T(8,128)(2,1)}) custom-call(bf16[224,512]{1,0:T(8,128)(2,1)} %tok.1, s32[2,224]{1,0:T(2,128)} %bitcast.9, f32[2,224]{1,0:T(2,128)} %bitcast.10, f32[1,32]{1,0:T(1,128)} %bitcast.11, ...), custom_call_target="tpu_custom_call" | custom-call | tf_op jit(solution)/shard_map/pallas_call | solution.py:379
  238.6 0.0 copy-start.1
  238.6 1.9 copy.15
  240.5 0.0 copy-done.1
  240.5 0.0 copy-start
  240.5 0.8 copy.16
  241.3 0.4 copy-done
  241.8 0.0 copy-start.2
  241.8 0.8 copy.17
  242.6 0.3 copy-done.2
  242.9 0.7 copy.18
Async XLA Ops:
  238.6 1.9 copy-start.1
  240.5 1.2 copy-start
  241.8 1.1 copy-start.2

commit v5 on v4

--- a/solution.py
+++ b/solution.py
@@ -282,6 +282,10 @@
         for j in range(1, T):
             remote(hb.at[p, tp], hb.at[p, tp], h_send, h_recv.at[p], tp_peer(j)).start()
 
+    def can_wait(to):
+        low, high = jnp.minimum(me, to), jnp.maximum(me, to)
+        return (high - low > S // 2) & (low >= S * 2 // 8)
+
     def send_back(d):
         back = lax.rem(S - d, S)
         remote(ob.at[d], ret.at[back], r_send, r_recv.at[back // rs], fs_peer(d)).start()
@@ -302,16 +306,22 @@
             ob[part, chunks] = y[s * half : (s + 1) * half].reshape(rs, MAIN, LANES).astype(bf16)
         near, far = ranges_of(p)
 
+        last = rs if near else rs - 1
+
         def send(i, c):
-            send_back(far * rs + i)
-            send_back(near * rs + rs - 1 - i)
+            for d in (far * rs + i, near * rs + rs - 1 - i):
+
+                @pl.when(jnp.logical_not(can_wait(lax.rem(me + d, S))))
+                def _():
+                    send_back(d)
+
             return c
 
-        if near:
-            lax.fori_loop(0, rs, send, 0)
-        else:
-            lax.fori_loop(0, rs - 1, send, 0)
-            send_back(far * rs + rs - 1)
+        lax.fori_loop(0, last, send, 0)
+        if not near:
+
+            send_back(S - 1)
+
             pltpu.make_async_copy(ob.at[0], ret.at[0], r_recv.at[0]).start()
 
     for p in range(PAIRS):
@@ -319,6 +329,17 @@
         if p + 1 < PAIRS:
             forward(p + 1)
         second_half(p)
+
+    def send_late(i, c):
+        d = far_first(i)
+
+        @pl.when(can_wait(lax.rem(me + d, S)))
+        def _():
+            send_back(d)
+
+        return c
+
+    lax.fori_loop(0, S - 1, send_late, 0)
 
     acc[...] = jnp.zeros_like(acc)
     for p in range(PAIRS):
@@ -359,6 +380,19 @@
     drain(ob.at[pl.ds(1, S - 1)], r_send)
     for a, ref in enumerate(outs):
         drain(w.at[a], out_sem.at[a])
+
+
+def settle(*refs):
+    n = (len(refs) - 2) // 3
+    sources, targets, held = refs[:n], refs[n : 2 * n], refs[2 * n : 3 * n]
+    in_sem, out_sem = refs[3 * n :]
+    for i in range(n):
+        pltpu.make_async_copy(sources[i], held[i], in_sem.at[i]).start()
+    for i in range(n):
+        pltpu.make_async_copy(sources[i], held[i], in_sem.at[i]).wait()
+        pltpu.make_async_copy(held[i], targets[i], out_sem.at[i]).start()
+    for i in range(n):
+        pltpu.make_async_copy(held[i], targets[i], out_sem.at[i]).wait()
 
 
 def local(shards, columns, groups, tokens, route_ids, route_weights, norm_gain, gate_m, up_m, down_m):
@@ -404,8 +438,14 @@
         ],
         compiler_params=pltpu.CompilerParams(collective_id=0, has_side_effects=True),
     )(tokens, route_ids.T, route_weights.T, norm_gain[None, :], gate_m, up_m, down_m)
-    gate, up, down = (o.reshape(1, S * depth, LANES) for o in outs[:3])
-    return gate, up, down, outs[3]
+    outs = [o.reshape(1, S * depth, LANES) for o in outs[:3]] + [outs[3]]
+    return pl.pallas_call(
+        settle,
+        out_shape=tuple(jax.ShapeDtypeStruct(o.shape, o.dtype) for o in outs),
+        in_specs=[anywhere] * len(outs),
+        out_specs=(anywhere,) * len(outs),
+        scratch_shapes=[pltpu.VMEM(o.shape, o.dtype) for o in outs] + [dma((len(outs),)), dma((len(outs),))],
+    )(*outs)
 
 
 def solution(mesh):

time: 244 us -> 239 us (0.980)
  local copies, waits for them, and re-layouts: 4.97 us -> 0 us
    unnamed x10 -> x0, local copies, waits for them, and re-layouts: 4.97 us -> none
where the time goes in v5:
time: 239 us
  Pallas kernels  238 us (100%)
    pallas_call x1, Pallas kernels, local(): pl.pallas_call(functools.partial(kernel, S, T, G), out_shape=(served, ser...  236 us

profile of v5, /device:TPU:33, one launch (start us, length us, event | category | flops | bytes accessed | tf_op | source)
XLA Modules:
  0.0 238.8 jit_solution(17156226506955778798)
XLA Ops:
  0.6 235.8 %shard_map.102 = (bf16[64,1,2,16,128]{4,3,2,1,0:T(8,128)(2,1)}, bf16[64,1,2,16,128]{4,3,2,1,0:T(8,128)(2,1)}, bf16[64,1,2,16,128]{4,3,2,1,0:T(8,128)(2,1)}, bf16[224,512]{1,0:T(8,128)(2,1)}) custom-call(bf16[224,512]{1,0:T(8,128)(2,1)} %tok.1, s32[2,224]{1,0:T(2,128)} %bitcast.9, f32[2,224]{1,0:T(2,128)} %bitcast.10, f32[1,32]{1,0:T(1,128)} %bitcast.11, ...), custom_call_target="tpu_custom_call" | custom-call | tf_op jit(solution)/shard_map/pallas_call | solution.py:413
  236.5 2.3 shard_map.103

commit v6 on v5

--- a/solution.py
+++ b/solution.py
@@ -140,8 +140,7 @@
         pltpu.make_async_copy(ws.at[0], w_mine, w_recv).start()
 
         def ship_before(i, c):
-            odd = lax.rem(i, 2)
-            ship(odd * (i // 2) + (1 - odd) * (place_of - 1 - i // 2))
+            ship(i)
             return c
 
         lax.fori_loop(0, place_of, ship_before, 0)

time: 239 us -> 240 us (level)
  no operation moved by 1% of the time
where the time goes in v6:
time: 240 us; the launch traced here: 239 us
  Pallas kernels  238 us (99%)
    pallas_call x1, Pallas kernels, local(): pl.pallas_call(functools.partial(kernel, S, T, G), out_shape=(served, ser...  236 us

profile of v6, /device:TPU:33, one launch (start us, length us, event | category | flops | bytes accessed | tf_op | source)
XLA Modules:
  0.0 239.0 jit_solution(13267332253340720015)
XLA Ops:
  0.6 236.0 %shard_map.102 = (bf16[64,1,2,16,128]{4,3,2,1,0:T(8,128)(2,1)}, bf16[64,1,2,16,128]{4,3,2,1,0:T(8,128)(2,1)}, bf16[64,1,2,16,128]{4,3,2,1,0:T(8,128)(2,1)}, bf16[224,512]{1,0:T(8,128)(2,1)}) custom-call(bf16[224,512]{1,0:T(8,128)(2,1)} %tok.1, s32[2,224]{1,0:T(2,128)} %bitcast.9, f32[2,224]{1,0:T(2,128)} %bitcast.10, f32[1,32]{1,0:T(1,128)} %bitcast.11, ...), custom_call_target="tpu_custom_call" | custom-call | tf_op jit(solution)/shard_map/pallas_call | solution.py:412
  236.7 2.3 shard_map.103
